TPU v7x, 32 devices: a whole 2x2x4 slice. The times are simulated.
32 devices in a mesh: sp: 8 (over z, x), tp: 4 (over y, core).
Axes of the slice: x: 2, y: 2, z: 4, core: 2. Of those that a mesh axis runs over, the one named last changes fastest.
Arguments:
- query_rows: bfloat16 [2048, 2048], P('sp', 'tp'), may hold values from -6 to 6
- key_rows: bfloat16 [2048, 2048], P('sp', 'tp'), may hold values from -6 to 6
- value_rows: bfloat16 [2048, 2048], P('sp', 'tp'), may hold values from -6 to 6
- gate_rows: bfloat16 [2048, 2048], P('sp', 'tp'), may hold values from -6 to 6
- log_decay: float32 [2048, 16], P('sp', 'tp'), may hold values from -1 to 0
- head_gain: float32 [2048], P('tp'), may hold values from 0.1 to 1.9
- out_weight: bfloat16 [2048, 2048], P('tp'), may hold values from -0.125 to 0.125
- residual: bfloat16 [2048, 2048], P(('sp', 'tp')), may hold values from -6 to 6
- ffn_gain: float32 [2048], replicated, may hold values from 0.1 to 1.9
- gate_weight: bfloat16 [8, 2048, 2048], P('sp', None, 'tp'), may hold values from -0.375 to 0.375
- up_weight: bfloat16 [8, 2048, 2048], P('sp', None, 'tp'), may hold values from -0.375 to 0.375
- down_weight: bfloat16 [8, 2048, 2048], P('sp', 'tp'), may hold values from -0.01953125 to 0.01953125
- routes: int32 [2048, 4], P('sp'), may hold values from 0 to 7, all different within a row; in each aligned block of 64 rows (0 to 63, 64 to 127, ...) at most 48 rows name the same one
- route_weights: float32 [2048, 4], P(('sp', 'tp')), may hold values from 0.05 to 1
Outputs:
- layer_out: bfloat16 [2048, 2048], P(('sp', 'tp'))
Inputs may be any that keep to these rules, and one draw needn't show every extreme that they name: `routes`: each row names 4 different experts. In each aligned block of 64 rows no expert is named by more than 48 rows, and in some block some expert is named by exactly 48 rows.
All inputs are finite; a program needn't handle non-finite values.
Results may differ from a plain program's by a relative error of at most 0.014.
Values may be sent and summed in bfloat16 or wider, within the bound.
A program may use at most 128 MiB of HBM per device.

v0:
```python
import jax
import jax.numpy as jnp
from jax import lax
from jax.sharding import PartitionSpec as P

HEAD_DIM = 128
TOPK = 4
BLOCK = 128


highest = lax.Precision.HIGHEST
rope_base = 10000.0
group_eps = 1e-05
square_eps = 1e-06
clamp_limit = 7.0
swish_alpha = 1.702


def entering_2(value, axis, join, neutral):
    count, mine = (lax.axis_size(axis), lax.axis_index(axis))
    pieces = jax.tree.map(lambda part: lax.all_gather(part, axis), value)
    total = jax.tree.map(
        lambda part, zero: jnp.full_like(part, 0) + jnp.asarray(zero, part.dtype), value, neutral
    )

    def turn(position, total):
        longer = join(total, jax.tree.map(lambda part: part[position], pieces))
        return jax.tree.map(lambda new, old: jnp.where(position < mine, new, old), longer, total)

    return lax.fori_loop(0, count - 1, turn, total)


def rotary_angles(positions, head_dim):
    half_dim = head_dim // 2
    inverse = rope_base ** (-jnp.arange(half_dim, dtype=jnp.float32) / half_dim)
    return positions[:, None] * inverse[None, :]


def rotate(values, angles):
    half_dim = values.shape[-1] // 2
    cosine = jnp.cos(angles)[:, None, :]
    sine_table = jnp.sin(angles)[:, None, :]
    first_half = values[..., :half_dim]
    second_half = values[..., half_dim:]
    return jnp.concatenate(
        [
            first_half * cosine - second_half * sine_table,
            second_half * cosine + first_half * sine_table,
        ],
        axis=-1,
    )


def block_pass(carry_state, queries, keys_rot, values, log_step):
    length = queries.shape[0]
    cumulative = jnp.cumsum(log_step, axis=0)
    gap_matrix = cumulative[:, None, :] - cumulative[None, :, :]
    causal = (
        jnp.arange(length, dtype=jnp.int32)[:, None] >= jnp.arange(length, dtype=jnp.int32)[None, :]
    )
    weights = jnp.where(causal[:, :, None], jnp.exp(jnp.minimum(gap_matrix, 0.0)), 0.0)
    scores = jnp.einsum("ihd,jhd->ijh", queries, keys_rot, precision=highest) * weights
    inner_part = jnp.einsum("ijh,jhe->ihe", scores, values, precision=highest)
    cross_part = (
        jnp.einsum("ihd,hde->ihe", queries, carry_state, precision=highest)
        * jnp.exp(cumulative)[:, :, None]
    )
    total_log = cumulative[-1]
    tail_weight = jnp.exp(total_log[None, :] - cumulative)
    carried = carry_state * jnp.exp(total_log)[:, None, None] + jnp.einsum(
        "jhd,jh,jhe->hde", keys_rot, tail_weight, values, precision=highest
    )
    return (carried, inner_part + cross_part)


def head_norm(retained, gain_row, gate_rows):
    mean_part = jnp.mean(retained, axis=-1, keepdims=True)
    centred = retained - mean_part
    variance = jnp.mean(centred * centred, axis=-1, keepdims=True)
    scaled = (centred * lax.rsqrt(variance + group_eps)).reshape(retained.shape[0], -1)
    return (scaled * gain_row * jax.nn.silu(gate_rows.astype(jnp.float32))).astype(jnp.bfloat16)


def square_norm(updated, gain_row):
    factor = lax.rsqrt(jnp.mean(updated * updated, axis=-1, keepdims=True) + square_eps)
    return (updated * factor * gain_row).astype(jnp.bfloat16)


def expert_rows(rows, gate_part, up_part):
    gate_pre = jnp.dot(rows, gate_part, preferred_element_type=jnp.float32)
    up_pre = jnp.dot(rows, up_part, preferred_element_type=jnp.float32)
    gate_clip = jnp.minimum(gate_pre, clamp_limit)
    up_clip = jnp.clip(up_pre, -clamp_limit, clamp_limit)
    return ((up_clip + 1.0) * (gate_clip * jax.nn.sigmoid(gate_clip * swish_alpha))).astype(
        jnp.bfloat16
    )


def slot_ranks(route_block, experts):
    flat_routes = route_block.reshape(-1)
    onehot = (flat_routes[:, None] == jnp.arange(experts, dtype=jnp.int32)[None, :]).astype(
        jnp.int32
    )
    return (flat_routes, jnp.sum(jnp.cumsum(onehot, axis=0) * onehot, axis=1) - 1)


def chain_pair(earlier_pair, later_pair):
    return (
        earlier_pair[0] * later_pair[0],
        later_pair[0][:, None, None] * earlier_pair[1] + later_pair[1],
    )


def body(
    query_rows,
    key_rows,
    value_rows,
    gate_rows,
    log_decay,
    head_gain,
    out_weight,
    residual,
    ffn_gain,
    gate_weight,
    up_weight,
    down_weight,
    routes,
    route_weights,
):
    tok_count = query_rows.shape[0]
    local_heads = log_decay.shape[1]
    sp_count = lax.axis_size("sp")
    tp_count = lax.axis_size("tp")
    model_width = residual.shape[1]
    rows_own = tok_count // tp_count
    capacity = max(2, 3 * rows_own * TOPK // (2 * sp_count))
    first_pos = lax.axis_index("sp") * tok_count
    positions = (first_pos + jnp.arange(tok_count, dtype=jnp.int32)).astype(jnp.float32)
    angles = rotary_angles(positions, HEAD_DIM)
    head_shape = (tok_count, local_heads, HEAD_DIM)
    queries = rotate(query_rows.astype(jnp.float32).reshape(head_shape), angles)
    keys_rot = rotate(key_rows.astype(jnp.float32).reshape(head_shape), angles) * HEAD_DIM ** (-0.5)
    values = value_rows.astype(jnp.float32).reshape(head_shape)
    block_count = tok_count // BLOCK

    def advance(carry_state, pieces):
        return block_pass(carry_state, pieces[0], pieces[1], pieces[2], pieces[3])

    start_state = jnp.zeros((local_heads, HEAD_DIM, HEAD_DIM), jnp.float32)
    block_shape = (block_count, BLOCK, local_heads, HEAD_DIM)
    local_state, retained = lax.scan(
        advance,
        start_state,
        (
            queries.reshape(block_shape),
            keys_rot.reshape(block_shape),
            values.reshape(block_shape),
            log_decay.reshape(block_count, BLOCK, local_heads),
        ),
    )
    retained = retained.reshape(head_shape)
    cumulative = jnp.cumsum(log_decay, axis=0)
    span_decay = jnp.exp(cumulative[-1])
    identity_pair = (jnp.ones((local_heads,), jnp.float32), jnp.zeros_like(local_state))
    entering = entering_2((span_decay, local_state), "sp", chain_pair, identity_pair)[1]
    retained = (
        retained
        + jnp.einsum("thd,hde->the", queries, entering, precision=highest)
        * jnp.exp(cumulative)[:, :, None]
    )
    hidden = head_norm(retained, head_gain, gate_rows)
    mixed_sum = lax.psum_scatter(
        jnp.dot(hidden, out_weight, preferred_element_type=jnp.float32).astype(jnp.bfloat16),
        "tp",
        scatter_dimension=0,
        tiled=True,
    ).astype(jnp.float32)
    updated = residual.astype(jnp.float32) + mixed_sum
    ffn_in = square_norm(updated, ffn_gain)
    tp_index = lax.axis_index("tp")
    own_routes = lax.dynamic_slice_in_dim(routes, tp_index * rows_own, rows_own, 0)
    own_experts, own_ranks = slot_ranks(own_routes, sp_count)
    home_slot = own_experts * capacity + own_ranks
    gate_part = gate_weight[0]
    up_part = up_weight[0]
    down_part = down_weight[0]
    empty_row = jnp.zeros((1, model_width), jnp.bfloat16)
    source_row = (
        jnp.full((sp_count * capacity,), rows_own, jnp.int32)
        .at[home_slot]
        .set(jnp.arange(rows_own * TOPK, dtype=jnp.int32) // TOPK)
    )
    padded = jnp.concatenate([ffn_in, empty_row], axis=0)
    outgoing = padded[source_row].reshape(sp_count, capacity, model_width)
    arrived = lax.all_to_all(outgoing, "sp", split_axis=0, concat_axis=0, tiled=True)
    fanned = lax.all_gather(arrived[None], "tp", axis=0, tiled=True)
    activity = expert_rows(fanned.reshape(-1, model_width), gate_part, up_part)
    partial_out = jnp.dot(activity, down_part, preferred_element_type=jnp.float32).reshape(
        tp_count, sp_count, capacity, model_width
    )
    summed = (
        lax.psum_scatter(partial_out.astype(jnp.bfloat16), "tp", scatter_dimension=0, tiled=True)
        .astype(jnp.float32)
        .reshape(sp_count, capacity, model_width)
    )
    returned = lax.all_to_all(
        summed.astype(jnp.bfloat16), "sp", split_axis=0, concat_axis=0, tiled=True
    )
    picked = returned.reshape(sp_count * capacity, model_width)[home_slot].reshape(
        rows_own, TOPK, model_width
    )
    expert_sum = jnp.sum(route_weights[:, :, None] * picked.astype(jnp.float32), axis=1)
    return (updated + expert_sum).astype(jnp.bfloat16)


def solution(mesh):
    return jax.shard_map(
        body,
        mesh=mesh,
        in_specs=(
            P("sp", "tp"),
            P("sp", "tp"),
            P("sp", "tp"),
            P("sp", "tp"),
            P("sp", "tp"),
            P("tp"),
            P("tp", None),
            P(("sp", "tp"), None),
            P(),
            P("sp", None, "tp"),
            P("sp", None, "tp"),
            P("sp", "tp", None),
            P("sp", None),
            P(("sp", "tp"), None),
        ),
        out_specs=P(("sp", "tp"), None),
        check_vma=False,
    )
```

profile of v0, /device:TPU:0, one launch (start us, length us, event | category | flops | bytes accessed | tf_op | source)
XLA Modules:
  0.0 369.0 jit_solution(12269270780117862284)
XLA Ops:
  6.6 1.3 copy.136
  7.9 1.0 copy.168
  8.9 1.0 copy.169
  10.1 1.0 copy.170
  11.1 1.0 copy.171
  12.1 0.5 multiply_cosine_fusion
  12.7 2.8 multiply_subtract_fusion
  15.5 2.0 copy.139
  17.5 1.9 copy.140
  19.4 1.9 reshape.225
  21.4 1.0 pad_maximum_fusion
  22.5 1.9 maximum_multiply_fusion
  24.3 29.0 %while.27 = (s32[]{:T(128)}, f32[4,128,128]{2,1,0:T(8,128)S(1)}, f32[2,128,4,128]{1,0,3,2:T(2,128)}, f32[2,128,4]{2,1,0:T(8,128)S(1)}, f32[2,128,4,128]{1,3,2,0:...) while((s32[]{:T(128)}, f32[4,128,128]{2,1,0:T(8,128)S(1)}, ...), condition=%wide.region_2.3_spmd.clone, body=%wide.region_0.2_spmd.clone.sunk | while | flops 403456000 | bytes 5312736 | solution.py:151
  24.3 0.2 reduce_window_sum.49
  24.6 1.6 fusion.77
  26.3 1.0 constant_dynamic-slice_fusion.4
  27.4 0.4 convolution_bitcast_fusion.5
  27.9 1.6 fusion.78
  29.5 7.6 %dynamic_update_slice.6 = f32[2,128,4,128]{1,0,3,2:T(2,128)} dynamic-update-slice(f32[2,128,4,128]{1,0,3,2:T(2,128)} %get-tuple-element.374, f32[1,128,4,128]{1,0,3,2:T(1,128)S(1)} %bitcast.143, s32[]{:T(128)} %get-tuple-element.372, s32[]{:T(128)} %constant.100.clone.1..sunk, s32[]{:T(128)} %constant.100.clone.1..sunk, s32[]{:T(128)} %constant.100.clone.1..sunk) | dynamic-update-slice | bytes 524292 | tf_op jit(solution)/shard_map/while/body/jit(dynamic_update_index_in_dim)/dynamic_update_slice | solution.py:151
  37.2 1.6 convolution_add_fusion.2
  38.9 0.2 reduce_window_sum.49
  39.1 1.6 fusion.77
  40.8 1.0 constant_dynamic-slice_fusion.4
  41.9 0.4 convolution_bitcast_fusion.5
  42.4 1.6 fusion.78
  44.0 7.6 %dynamic_update_slice.6 = f32[2,128,4,128]{1,0,3,2:T(2,128)} dynamic-update-slice(f32[2,128,4,128]{1,0,3,2:T(2,128)} %get-tuple-element.374, f32[1,128,4,128]{1,0,3,2:T(1,128)S(1)} %bitcast.143, s32[]{:T(128)} %get-tuple-element.372, s32[]{:T(128)} %constant.100.clone.1..sunk, s32[]{:T(128)} %constant.100.clone.1..sunk, s32[]{:T(128)} %constant.100.clone.1..sunk) | dynamic-update-slice | bytes 524292 | tf_op jit(solution)/shard_map/while/body/jit(dynamic_update_index_in_dim)/dynamic_update_slice | solution.py:151
  51.7 1.6 convolution_add_fusion.2
  53.4 0.7 copy-done.1
  54.2 1.2 reduce-window.14
  55.8 1.5 reshape.215
  57.3 0.2 fusion.40
  57.4 22.3 %all-gather.2 = f32[8,1,4]{2,1,0:T(1,128)S(1)} all-gather(f32[1,1,4]{2,1,0:T(1,128)S(1)} %bitcast.160), channel_id=1, replica_groups=mesh['sp'=8,'tp'=4] {'sp'}, dimensions={0}, use_global_device_ids=true | all-gather | bytes 144 | tf_op jit(solution)/shard_map/all_gather | solution.py:21
  79.7 26.4 %all-gather.6.cloned.1.call-done = f32[32,128,128]{2,1,0:T(8,128)} async-done(((f32[4,128,128]{2,1,0:T(8,128)}), f32[32,128,128]{2,1,0:T(8,128)}) %all-gather.6.cloned.1.call-update) | async-done | bytes 2097168 | tf_op jit(solution)/shard_map/all_gather | solution.py:21
  106.2 7.6 %while.28 = (s32[]{:T(128)}, f32[4,128,128]{2,1,0:T(8,128)S(1)}, s32[]{:T(128)}, f32[8,4]{1,0:T(8,128)S(1)}, f32[8,4,128,128]{3,2,1,0:T(8,128)}, /*index=5*/s32[]{:T(128)}, s32[]{:T(128)}) while((s32[]{:T(128)}, f32[4,128,128]{2,1,0:T(8,128)S(1)}, s32[]{:T(128)}, f32[8,4]{1,0:T(8,128)S(1)}, f32[8,4,128,128]{3,2,1,0:T(8,128)}, ...), condition=%wide.region_6.7_spmd.clone, body=%wide.region_5.6_spmd.clone.sunk | while | flops 262148 | bytes 786585 | solution.py:30
  106.2 1.0 fusion.79
  107.2 1.1 fusion.79
  108.3 1.1 fusion.79
  109.4 1.1 fusion.79
  110.5 1.1 fusion.79
  111.6 1.1 fusion.79
  112.7 1.1 fusion.79
  113.8 1.7 fusion.48
  115.6 0.2 copy.152
  115.9 3.5 convolution_convert_fusion.1
  119.9 0.6 reduce-window.16
  120.5 0.2 slice_reduce_fusion
  121.0 1.4 scatter_custom_fusion
  122.5 20.5 %reduce-scatter.3.cloned.1.call-done = bf16[64,2048]{1,0:T(8,128)(2,1)} async-done(((bf16[256,2048]{1,0:T(8,128)(2,1)}), bf16[64,2048]{1,0:T(8,128)(2,1)}) %reduce-scatter.3.cloned.1.call-update) | async-done | bytes 262160 | tf_op jit(solution)/shard_map/reduce_scatter | solution.py:172
  142.9 1.1 multiply_reduce_fusion.1
  144.1 1.1 multiply_convert_fusion
  145.2 3.1 gather_fusion
  148.3 42.4 %all_to_all.10 = bf16[8,48,2048]{2,1,0:T(8,128)(2,1)} all-to-all(bf16[8,48,2048]{2,1,0:T(8,128)(2,1)} %bitcast.144), channel_id=1, replica_groups=mesh['sp'=8,'tp'=4] {'sp'}, dimensions={0} | all-to-all | bytes 3145728 | tf_op jit(solution)/shard_map/all_to_all | solution.py:195
  190.8 0.2 reduce-scatter.5.cloned.1.call-start
  191.0 44.4 %all-gather.8.cloned.1.call-done = bf16[32,48,2048]{2,1,0:T(8,128)(2,1)} async-done(((bf16[8,48,2048]{2,1,0:T(8,128)(2,1)}), bf16[32,48,2048]{2,1,0:T(8,128)(2,1)}) %all-gather.8.cloned.1.call-update) | async-done | bytes 6291472 | tf_op jit(solution)/shard_map/all_gather | solution.py:196
  235.4 6.3 %convolution_minimum_fusion = f32[1536,512]{1,0:T(8,128)S(1)} fusion(bf16[1536,2048]{1,0:T(8,128)(2,1)} %bitcast.161, bf16[1,2048,512]{2,1,0:T(8,128)(2,1)} %param.27), kind=kOutput, calls=%fused_computation.39 | convolution fusion | flops 3222011904 | bytes 11534336 | tf_op jit(solution)/shard_map/dot_general | solution.py:90
  241.7 4.1 %fusion.24 = bf16[1536,512]{1,0:T(8,128)(2,1)S(1)} fusion(f32[1536,512]{1,0:T(8,128)S(1)} %convolution_minimum_fusion, bf16[1536,2048]{1,0:T(8,128)(2,1)S(1)} %bitcast.162, bf16[1,2048,512]{2,1,0:T(8,128)(2,1)S(1)} %copy-done.10), kind=kOutput, calls=%fused_computation.42 | convolution fusion | flops 3228303360 | bytes 13107200 | tf_op jit(solution)/shard_map/dot_general | solution.py:91
  245.8 5.4 %convolution_convert_fusion = bf16[4,8,48,2048]{3,2,1,0:T(8,128)(2,1)} fusion(bf16[4,8,48,512]{3,2,1,0:T(8,128)(2,1)S(1)} %bitcast.163, bf16[1,512,2048]{2,1,0:T(8,128)(2,1)S(1)} %copy-done), kind=kOutput, calls=%fused_computation.37 | convolution fusion | flops 3224371200 | bytes 9961472 | tf_op jit(solution)/shard_map/dot_general | solution.py:198
  251.2 59.0 %reduce-scatter.5.cloned.1.call-done = bf16[1,8,48,2048]{3,2,1,0:T(8,128)(2,1)} async-done(((bf16[4,8,48,2048]{3,2,1,0:T(8,128)(2,1)}), bf16[1,8,48,2048]{3,2,1,0:T(8,128)(2,1)}) %reduce-scatter.5.cloned.1.call-update) | async-done | bytes 1572880 | tf_op jit(solution)/shard_map/reduce_scatter | solution.py:202
  310.2 5.5 %all-to-all-start.1 = ((bf16[8,48,2048]{2,1,0:T(8,128)(2,1)}), bf16[8,48,2048]{2,1,0:T(8,128)(2,1)}, u32[]{:S(2)}, u32[]{:S(2)}) async-start(bf16[8,48,2048]{2,1,0:T(8,128)(2,1)} %bitcast.151), calls=%async_computation.3 | async-start | bytes 3145728 | tf_op jit(solution)/shard_map/all_to_all | solution.py:206
  315.9 36.8 %all-to-all-done.1 = bf16[8,48,2048]{2,1,0:T(8,128)(2,1)} async-done(((bf16[8,48,2048]{2,1,0:T(8,128)(2,1)}), bf16[8,48,2048]{2,1,0:T(8,128)(2,1)}, u32[]{:S(2)}, u32[]{:S(2)}) %all-to-all-start.1) | async-done | bytes 1572896 | tf_op jit(solution)/shard_map/all_to_all | solution.py:206
  352.7 4.0 %gather_fusion.1 = bf16[256,2048]{1,0:T(8,128)(2,1)S(1)} fusion(bf16[384,2048]{1,0:T(8,128)(2,1)} %bitcast.28, s32[1024]{0:T(1024)S(1)} %pad_clamp_fusion), kind=kCustom, calls=%fused_computation.1 | custom fusion | bytes 2098176 | tf_op jit(solution)/shard_map/gather | solution.py:209
  356.7 1.7 reshape.228
  358.4 3.2 multiply_reduce_fusion
  361.6 0.8 add_convert_fusion
  (96 shorter events, 2.8 us)
Async XLA Ops:
  6.5 239.3 %copy-start = (bf16[1,512,2048]{2,1,0:T(8,128)(2,1)S(1)}, bf16[1,512,2048]{2,1,0:T(8,128)(2,1)}, u32[]{:S(2)}) copy-start(bf16[1,512,2048]{2,1,0:T(8,128)(2,1)} %param.29) | copy-start | bytes 6291460
  6.5 3.4 copy-start.4
  6.5 99.6 %all-gather.6.cloned.1.call-start = ((), (), s32[]{:S(2)}) async-start(), calls=%async_computation.6 | async-start | bytes 2359296 | tf_op jit(solution)/shard_map/all_gather | solution.py:21
  15.5 5.8 %copy-start.5 = (f32[256,4]{0,1:T(4,128)S(1)}, f32[256,4]{0,1:T(4,128)}, u32[]{:S(2)}) copy-start(f32[256,4]{0,1:T(4,128)} %param.22) | copy-start | bytes 12292
  53.4 0.7 copy-start.1
  54.1 88.8 %reduce-scatter.3.cloned.1.call-start = ((), (), s32[]{:S(2)}) async-start(), calls=%async_computation.4 | async-start | bytes 1310720 | tf_op jit(solution)/shard_map/reduce_scatter | solution.py:172
  113.8 2.1 copy-start.11
  115.9 3.6 copy-start.8
  115.9 27.0 %copy-start.2 = (bf16[64,2048]{1,0:T(8,128)(2,1)S(1)}, bf16[64,2048]{1,0:T(8,128)(2,1)}, u32[]{:S(2)}) copy-start(bf16[64,2048]{1,0:T(8,128)(2,1)} %param.25) | copy-start | bytes 786436
  115.9 28.2 %copy-start.6 = (f32[2048]{0:T(1024)S(1)}, f32[2048]{0:T(1024)}, u32[]{:S(2)}) copy-start(f32[2048]{0:T(1024)} %param.26) | copy-start | bytes 24580
  119.4 116.0 %all-gather.8.cloned.1.call-start = ((), (), s32[]{:S(2)}) async-start(), calls=%async_computation.7 | async-start | bytes 7864320 | tf_op jit(solution)/shard_map/all_gather | solution.py:196
  190.8 119.5 %reduce-scatter.5.cloned.1.call-start = ((), (), s32[]{:S(2)}) async-start(), calls=%async_computation.5 | async-start | bytes 7864320 | tf_op jit(solution)/shard_map/reduce_scatter | solution.py:202
  235.4 6.3 %copy-start.9 = (bf16[32,48,2048]{2,1,0:T(8,128)(2,1)S(1)}, bf16[32,48,2048]{2,1,0:T(8,128)(2,1)}, u32[]{:S(2)}) copy-start(bf16[32,48,2048]{2,1,0:T(8,128)(2,1)} %all-gather.8.cloned.1.call-done) | copy-start | bytes 18874372
  235.4 6.3 %copy-start.10 = (bf16[1,2048,512]{2,1,0:T(8,128)(2,1)S(1)}, bf16[1,2048,512]{2,1,0:T(8,128)(2,1)}, u32[]{:S(2)}) copy-start(bf16[1,2048,512]{2,1,0:T(8,128)(2,1)} %param.28) | copy-start | bytes 6291460
  251.2 64.5 %copy-start.7 = (f32[64,4]{0,1:T(4,128)S(1)}, f32[64,4]{0,1:T(4,128)}, u32[]{:S(2)}) copy-start(f32[64,4]{0,1:T(4,128)} %param.31) | copy-start | bytes 3076
  310.2 42.5 %all-to-all-start.1 = ((bf16[8,48,2048]{2,1,0:T(8,128)(2,1)}), bf16[8,48,2048]{2,1,0:T(8,128)(2,1)}, u32[]{:S(2)}, u32[]{:S(2)}) async-start(bf16[8,48,2048]{2,1,0:T(8,128)(2,1)} %bitcast.151), calls=%async_computation.3 | async-start | bytes 3145728 | tf_op jit(solution)/shard_map/all_to_all | solution.py:206
  358.4 3.2 copy-start.3
Sparse Core Ops, SparseCore 0:
  54.2 51.8 all-gather.5
  119.5 23.3 reduce-scatter.2
  190.9 44.4 all-gather.7
  251.3 58.8 reduce-scatter.4
where the time goes:
time: 371 us; the launch traced here: 369 us
  waiting for transfers between devices  187 us (50%)
  blocking collectives  64.7 us (17%)
  local copies, waits for them, and re-layouts  43.4 us (12%)
  matrix products  31.5 us (8%)
  other arithmetic  22.6 us (6%)
  between operations  13.5 us (4%)
  starting transfers between devices  5.83 us (2%)
    reduce_scatter x1, waiting for transfers between devices, body(): lax.psum_scatter(partial_out.astype(jnp.bfloat16), 'tp', scatter_dimensio...  59 us
    all_gather x1, waiting for transfers between devices, body(): fanned = lax.all_gather(arrived[None], 'tp', axis=0, tiled=True)  44.4 us
    all_to_all x1, blocking collectives, body(): lax.all_to_all(outgoing, 'sp', split_axis=0, concat_axis=0, tiled=True)  42.4 us
    all_to_all x1, waiting for transfers between devices, body(): lax.all_to_all(summed.astype(jnp.bfloat16), 'sp', split_axis=0, concat_ax...  36.8 us
    all_gather x1, waiting for transfers between devices, entering_2(): pieces = jax.tree.map(lambda part: lax.all_gather(part, axis), value)  26.4 us
    all_gather x1, blocking collectives, entering_2(): pieces = jax.tree.map(lambda part: lax.all_gather(part, axis), value)  22.3 us
    reduce_scatter x1, waiting for transfers between devices, body(): lax.psum_scatter(jnp.dot(hidden, out_weight, preferred_element_type=jnp.f...  20.5 us
    dynamic_update_slice x2, local copies, waits for them, and re-layouts, body(): lax.scan(advance, start_state, (queries.reshape(block_shape), keys_rot.re...  15.3 us
  transfers between devices with their start and end apart: 5, of which 5 were waited for; matrix products, arithmetic and copies ran while one was open for 2% of the time, Pallas kernels for 0%

commit v1 on v0

v1 whole, which is shorter than its diff:
```python
import functools

import jax
import jax.numpy as jnp
from jax import lax
from jax.experimental import pallas as pl
from jax.experimental.pallas import tpu as pltpu
from jax.sharding import PartitionSpec as P

HEAD_DIM = 128
TOPK = 4
BLOCK = 128


highest = lax.Precision.HIGHEST
rope_base = 10000.0
group_eps = 1e-05
square_eps = 1e-06
clamp_limit = 7.0
swish_alpha = 1.702


def rotary_angles(positions, head_dim):
    half_dim = head_dim // 2
    inverse = rope_base ** (-jnp.arange(half_dim, dtype=jnp.float32) / half_dim)
    return positions[:, None] * inverse[None, :]


def square_norm(updated, gain_row):
    factor = lax.rsqrt(jnp.mean(updated * updated, axis=-1, keepdims=True) + square_eps)
    return (updated * factor * gain_row).astype(jnp.bfloat16)


def expert_rows(rows, gate_part, up_part):
    gate_pre = jnp.dot(rows, gate_part, preferred_element_type=jnp.float32)
    up_pre = jnp.dot(rows, up_part, preferred_element_type=jnp.float32)
    gate_clip = jnp.minimum(gate_pre, clamp_limit)
    up_clip = jnp.clip(up_pre, -clamp_limit, clamp_limit)
    return ((up_clip + 1.0) * (gate_clip * jax.nn.sigmoid(gate_clip * swish_alpha))).astype(
        jnp.bfloat16
    )


def slot_ranks(route_block, experts):
    flat_routes = route_block.reshape(-1)
    onehot = (flat_routes[:, None] == jnp.arange(experts, dtype=jnp.int32)[None, :]).astype(
        jnp.int32
    )
    return (flat_routes, jnp.sum(jnp.cumsum(onehot, axis=0) * onehot, axis=1) - 1)


def retention_kernel(q_ref, k_ref, v_ref, cos_ref, sin_ref, cum_ref, cum_row_ref, ret_ref, qdec_ref, state_ref):
    head = pl.program_id(0)
    length = q_ref.shape[0]
    cosine, sine = cos_ref[...], sin_ref[...]
    half = HEAD_DIM // 2

    def turned(ref):
        rows = ref[...].astype(jnp.float32)
        return rows * cosine + pltpu.roll(rows, half, 1) * sine

    lanes = lax.broadcasted_iota(jnp.int32, cum_ref.shape, 1)
    column = jnp.sum(jnp.where(lanes == head, cum_ref[...], 0.0), axis=1, keepdims=True)
    row = cum_row_ref[0]
    queries = turned(q_ref)
    keys = turned(k_ref) * HEAD_DIM ** (-0.5)
    values = v_ref[...]
    scores = lax.dot_general(
        queries.astype(jnp.bfloat16),
        keys.astype(jnp.bfloat16),
        (((1,), (1,)), ((), ())),
        preferred_element_type=jnp.float32,
    )
    causal = lax.broadcasted_iota(jnp.int32, (length, length), 0) >= lax.broadcasted_iota(
        jnp.int32, (length, length), 1
    )
    weights = jnp.where(causal, jnp.exp(jnp.minimum(column - row, 0.0)), 0.0)
    ret_ref[...] = jnp.dot(
        (scores * weights).astype(jnp.bfloat16), values, preferred_element_type=jnp.float32
    )
    qdec_ref[...] = (queries * jnp.exp(column)).astype(jnp.bfloat16)
    total = column[length - 1 :, :]
    tailed = (keys * jnp.exp(total - column)).astype(jnp.bfloat16)
    state_ref[0, :HEAD_DIM, :] = lax.dot_general(
        tailed, values, (((0,), (0,)), ((), ())), preferred_element_type=jnp.float32
    )
    state_ref[0, HEAD_DIM:, :] = jnp.broadcast_to(total, (8, HEAD_DIM))


def norm_kernel(ret_ref, qdec_ref, enter_ref, gain_ref, gate_ref, hidden_ref):
    retained = ret_ref[...] + jnp.dot(
        qdec_ref[...], enter_ref[0].astype(jnp.bfloat16), preferred_element_type=jnp.float32
    )
    centred = retained - jnp.mean(retained, axis=-1, keepdims=True)
    variance = jnp.mean(centred * centred, axis=-1, keepdims=True)
    gate = gate_ref[...].astype(jnp.float32)
    scaled = centred * lax.rsqrt(variance + group_eps) * gain_ref[...]
    hidden_ref[...] = (scaled * (gate / (1.0 + jnp.exp(-gate)))).astype(jnp.bfloat16)


def retention(query_rows, key_rows, value_rows, gate_rows, log_decay, head_gain):
    length, local_heads = log_decay.shape
    width = query_rows.shape[1]
    sp_count, mine = lax.axis_size("sp"), lax.axis_index("sp")
    positions = (mine * length + jnp.arange(length, dtype=jnp.int32)).astype(jnp.float32)
    angles = rotary_angles(positions, HEAD_DIM)
    cosine, sine = jnp.cos(angles), jnp.sin(angles)
    cosine = jnp.concatenate([cosine, cosine], axis=1)
    sine = jnp.concatenate([-sine, sine], axis=1)
    cumulative = jnp.cumsum(log_decay, axis=0)
    rows_spec = pl.BlockSpec((length, HEAD_DIM), lambda h: (0, h))
    table_spec = pl.BlockSpec((length, HEAD_DIM), lambda h: (0, 0))
    retained, qdec, state = pl.pallas_call(
        retention_kernel,
        grid=(local_heads,),
        out_shape=(
            jax.ShapeDtypeStruct((length, width), jnp.float32),
            jax.ShapeDtypeStruct((length, width), jnp.bfloat16),
            jax.ShapeDtypeStruct((local_heads, HEAD_DIM + 8, HEAD_DIM), jnp.float32),
        ),
        in_specs=[
            rows_spec,
            rows_spec,
            rows_spec,
            table_spec,
            table_spec,
            pl.BlockSpec((length, local_heads), lambda h: (0, 0)),
            pl.BlockSpec((1, 1, length), lambda h: (h, 0, 0)),
        ],
        out_specs=(
            rows_spec,
            rows_spec,
            pl.BlockSpec((1, HEAD_DIM + 8, HEAD_DIM), lambda h: (h, 0, 0)),
        ),
    )(query_rows, key_rows, value_rows, cosine, sine, cumulative, cumulative.T[:, None, :])
    pieces = lax.all_gather(state, "sp")
    totals = pieces[:, :, HEAD_DIM, 0]
    index = jnp.arange(sp_count, dtype=jnp.int32)
    between = (index[None, :] > index[:, None]) & (index[None, :] < mine)
    gap = jnp.sum(jnp.where(between[:, :, None], totals[None], 0.0), axis=1)
    factor = jnp.where((index < mine)[:, None], jnp.exp(gap), 0.0)
    entering = jnp.sum(factor[:, :, None, None] * pieces[:, :, :HEAD_DIM, :], axis=0)
    return pl.pallas_call(
        norm_kernel,
        grid=(local_heads,),
        out_shape=jax.ShapeDtypeStruct((length, width), jnp.bfloat16),
        in_specs=[
            rows_spec,
            rows_spec,
            pl.BlockSpec((1, HEAD_DIM, HEAD_DIM), lambda h: (h, 0, 0)),
            pl.BlockSpec((1, HEAD_DIM), lambda h: (0, h)),
            rows_spec,
        ],
        out_specs=rows_spec,
    )(retained, qdec, entering, head_gain[None, :], gate_rows)


def dense_experts(updated, ffn_in, own_routes, route_weights, gate_part, up_part, down_part):
    sp_count, mine = lax.axis_size("sp"), lax.axis_index("sp")
    width = ffn_in.shape[1]
    chosen = own_routes[:, :, None] == jnp.arange(sp_count, dtype=jnp.int32)[None, None, :]
    shares = jnp.sum(jnp.where(chosen, route_weights[:, :, None], 0.0), axis=1)
    coarse = shares.astype(jnp.bfloat16)
    fine = (shares - coarse.astype(jnp.float32)).astype(jnp.bfloat16)
    spare = jnp.zeros((ffn_in.shape[0], 128 - 2 * sp_count), jnp.bfloat16)
    payload = jnp.concatenate([ffn_in, coarse, fine, spare], axis=1)
    everyone = lax.all_gather(payload, ("sp", "tp"), axis=0, tiled=True)
    rows = everyone[:, :width]
    tail = everyone[:, width:].astype(jnp.float32)
    lane = jnp.arange(128, dtype=jnp.int32)[None, :]
    weight = jnp.sum(
        jnp.where((lane == mine) | (lane == mine + sp_count), tail, 0.0), axis=1, keepdims=True
    )
    activity = expert_rows(rows, gate_part, up_part)
    partial_out = jnp.dot(activity, down_part, preferred_element_type=jnp.float32) * weight
    summed = lax.psum_scatter(
        partial_out.astype(jnp.bfloat16), ("sp", "tp"), scatter_dimension=0, tiled=True
    )
    return (updated + summed.astype(jnp.float32)).astype(jnp.bfloat16)


def body(
    query_rows,
    key_rows,
    value_rows,
    gate_rows,
    log_decay,
    head_gain,
    out_weight,
    residual,
    ffn_gain,
    gate_weight,
    up_weight,
    down_weight,
    routes,
    route_weights,
):
    tok_count = query_rows.shape[0]
    local_heads = log_decay.shape[1]
    sp_count = lax.axis_size("sp")
    tp_count = lax.axis_size("tp")
    model_width = residual.shape[1]
    rows_own = tok_count // tp_count
    capacity = max(2, 3 * rows_own * TOPK // (2 * sp_count))
    hidden = retention(query_rows, key_rows, value_rows, gate_rows, log_decay, head_gain)
    mixed_sum = lax.psum_scatter(
        jnp.dot(hidden, out_weight, preferred_element_type=jnp.float32).astype(jnp.bfloat16),
        "tp",
        scatter_dimension=0,
        tiled=True,
    ).astype(jnp.float32)
    updated = residual.astype(jnp.float32) + mixed_sum
    ffn_in = square_norm(updated, ffn_gain)
    tp_index = lax.axis_index("tp")
    own_routes = lax.dynamic_slice_in_dim(routes, tp_index * rows_own, rows_own, 0)
    if rows_own < 2 * capacity and 2 * sp_count <= 128:
        return dense_experts(
            updated, ffn_in, own_routes, route_weights, gate_weight[0], up_weight[0], down_weight[0]
        )
    own_experts, own_ranks = slot_ranks(own_routes, sp_count)
    home_slot = own_experts * capacity + own_ranks
    gate_part = gate_weight[0]
    up_part = up_weight[0]
    down_part = down_weight[0]
    empty_row = jnp.zeros((1, model_width), jnp.bfloat16)
    source_row = (
        jnp.full((sp_count * capacity,), rows_own, jnp.int32)
        .at[home_slot]
        .set(jnp.arange(rows_own * TOPK, dtype=jnp.int32) // TOPK)
    )
    padded = jnp.concatenate([ffn_in, empty_row], axis=0)
    outgoing = padded[source_row].reshape(sp_count, capacity, model_width)
    arrived = lax.all_to_all(outgoing, "sp", split_axis=0, concat_axis=0, tiled=True)
    fanned = lax.all_gather(arrived[None], "tp", axis=0, tiled=True)
    activity = expert_rows(fanned.reshape(-1, model_width), gate_part, up_part)
    partial_out = jnp.dot(activity, down_part, preferred_element_type=jnp.float32).reshape(
        tp_count, sp_count, capacity, model_width
    )
    summed = (
        lax.psum_scatter(partial_out.astype(jnp.bfloat16), "tp", scatter_dimension=0, tiled=True)
        .astype(jnp.float32)
        .reshape(sp_count, capacity, model_width)
    )
    returned = lax.all_to_all(
        summed.astype(jnp.bfloat16), "sp", split_axis=0, concat_axis=0, tiled=True
    )
    picked = returned.reshape(sp_count * capacity, model_width)[home_slot].reshape(
        rows_own, TOPK, model_width
    )
    expert_sum = jnp.sum(route_weights[:, :, None] * picked.astype(jnp.float32), axis=1)
    return (updated + expert_sum).astype(jnp.bfloat16)


def solution(mesh):
    return jax.shard_map(
        body,
        mesh=mesh,
        in_specs=(
            P("sp", "tp"),
            P("sp", "tp"),
            P("sp", "tp"),
            P("sp", "tp"),
            P("sp", "tp"),
            P("tp"),
            P("tp", None),
            P(("sp", "tp"), None),
            P(),
            P("sp", None, "tp"),
            P("sp", None, "tp"),
            P("sp", "tp", None),
            P("sp", None),
            P(("sp", "tp"), None),
        ),
        out_specs=P(("sp", "tp"), None),
        check_vma=False,
    )
```

time: 371 us -> 371 us (level)
  waiting for transfers between devices: 187 us -> 305 us
  blocking collectives: 64.7 us -> 0 us
  local copies, waits for them, and re-layouts: 43.4 us -> 4.16 us
  other arithmetic: 22.6 us -> 10.6 us
  Pallas kernels: 0 us -> 8.27 us
  starting transfers between devices: 5.83 us -> 0.13 us
    reduce_scatter x1, waiting for transfers between devices: 59 us -> 149 us  [dense_experts(): lax.psum_scatter(partial_out.astype(jnp.bfloat16), ('sp', 'tp'), scatter_...]
    all_gather x2, waiting for transfers between devices: 70.8 us -> 132 us  [the longest x1 79.2 us: dense_experts(): everyone = lax.all_gather(payload, ('sp', 'tp'), axis=0, tiled=True)]
    all_to_all x1 -> x0, blocking collectives: 42.4 us -> none  [body(): lax.all_to_all(outgoing, 'sp', split_axis=0, concat_axis=0, tiled=True)]
    all_to_all x1 -> x0, waiting for transfers between devices: 36.8 us -> none  [body(): lax.all_to_all(summed.astype(jnp.bfloat16), 'sp', split_axis=0, concat_ax...]
    all_gather x1 -> x0, blocking collectives: 22.3 us -> none  [entering_2(): pieces = jax.tree.map(lambda part: lax.all_gather(part, axis), value)]
    dynamic_update_slice x2 -> x0, local copies, waits for them, and re-layouts: 15.3 us -> none  [body(): lax.scan(advance, start_state, (queries.reshape(block_shape), keys_rot.re...]
    pallas_call x0 -> x2, Pallas kernels: none -> 8.27 us  [the longest x1 4.32 us: retention(): pl.pallas_call(retention_kernel, grid=(local_heads,), out_shape=(jax.Shap...]
    select_n x10 -> x1, other arithmetic: 7.38 us -> 0.01 us  [retention(): factor = jnp.where((index < mine)[:, None], jnp.exp(gap), 0.0)]
  transfers between devices with their start and end apart: 5 -> 4, of which waited for: 5 -> 4; matrix products, arithmetic and copies ran while one was open for 2% -> 0% of each run, Pallas kernels for 0% -> 0%
where the time goes in v1:
time: 371 us; the launch traced here: 370 us
  waiting for transfers between devices  305 us (82%)
  matrix products  29.1 us (8%)
  between operations  13.2 us (4%)
  other arithmetic  10.6 us (3%)
  Pallas kernels  8.27 us (2%)
  local copies, waits for them, and re-layouts  4.16 us (1%)
    reduce_scatter x1, waiting for transfers between devices, dense_experts(): lax.psum_scatter(partial_out.astype(jnp.bfloat16), ('sp', 'tp'), scatter_...  149 us
    all_gather x1, waiting for transfers between devices, dense_experts(): everyone = lax.all_gather(payload, ('sp', 'tp'), axis=0, tiled=True)  79.2 us
    all_gather x1, waiting for transfers between devices, retention(): pieces = lax.all_gather(state, 'sp')  53.2 us
    reduce_scatter x1, waiting for transfers between devices, body(): lax.psum_scatter(jnp.dot(hidden, out_weight, preferred_element_type=jnp.f...  23.1 us
    dot_general x1, matrix products, dense_experts(): jnp.dot(activity, down_part, preferred_element_type=jnp.float32) * weight  15.2 us
    dot_general x1, matrix products, expert_rows(): gate_pre = jnp.dot(rows, gate_part, preferred_element_type=jnp.float32)  10.5 us
  transfers between devices with their start and end apart: 4, of which 4 were waited for; matrix products, arithmetic and copies ran while one was open for 0% of the time, Pallas kernels for 0%

profile of v1, /device:TPU:0, one launch (start us, length us, event | category | flops | bytes accessed | tf_op | source)
XLA Modules:
  0.0 370.2 jit_solution(9495550698441821138)
XLA Ops:
  6.5 0.0 copy-start
  6.5 0.0 all-gather.6.cloned.1.call-start
  6.6 0.8 reshape.110
  7.4 1.2 reduce-window.6
  8.6 0.1 slice.24
  8.7 0.1 copy.36
  8.8 0.1 copy.37
  8.9 0.1 broadcast_add_fusion
  9.0 0.0 copy-start.3
  9.0 0.8 copy.38
  9.8 0.5 fusion.18
  10.4 0.8 pad_maximum_fusion
  11.2 0.0 copy-done.3
  11.2 4.3 %shard_map.136 = (f32[256,512]{1,0:T(8,128)}, bf16[256,512]{1,0:T(8,128)(2,1)}, f32[4,136,128]{2,1,0:T(8,128)}) custom-call(bf16[256,512]{1,0:T(8,128)(2,1)} %q_ref.1, bf16[256,512]{1,0:T(8,128)(2,1)} %k_ref.1, bf16[256,512]{1,0:T(8,128)(2,1)} %v_ref.1, f32[256,128]{1,0:T(8,128)} %get-tuple-element.16.cos_ref, f32[256,128]{1,0:T(8,128)} %get-tuple-element.17.sin_ref, ...), custom_call_target="tpu_custom_call" | custom-call | tf_op jit(solution)/shard_map/pallas_call | solution.py:113
  15.5 0.0 all-gather.6.cloned.1.call-update
  15.5 0.0 reduce-scatter.3.cloned.1.call-start
  15.6 53.2 %all-gather.6.cloned.1.call-done = f32[32,136,128]{2,1,0:T(8,128)} async-done(((f32[4,136,128]{2,1,0:T(8,128)}), f32[32,136,128]{2,1,0:T(8,128)}) %all-gather.6.cloned.1.call-update) | async-done | bytes 2228240 | tf_op jit(solution)/shard_map/all_gather | solution.py:136
  68.8 0.9 slice.25
  69.7 0.1 copy.43
  69.8 0.1 select_reduce_fusion.2
  69.9 0.1 copy.40
  70.0 0.0 copy-start.6
  70.0 0.0 copy-start.5
  70.0 0.0 copy-start.1
  70.0 0.0 copy-start.4
  70.0 2.6 fusion.6.enter_ref
  72.6 4.0 %shard_map.137 = bf16[256,512]{1,0:T(8,128)(2,1)} custom-call(f32[256,512]{1,0:T(8,128)} %get-tuple-element.8.ret_ref, bf16[256,512]{1,0:T(8,128)(2,1)} %get-tuple-element.9.qdec_ref, f32[4,128,128]{2,1,0:T(8,128)} %fusion.6.enter_ref, f32[1,512]{1,0:T(1,128)} %bitcast.29, bf16[256,512]{1,0:T(8,128)(2,1)} %gate_ref.1), custom_call_target="tpu_custom_call" | custom-call | tf_op jit(solution)/shard_map/pallas_call | solution.py:143
  76.6 3.4 convolution_convert_fusion
  80.0 0.0 reduce-scatter.3.cloned.1.call-update
  80.0 0.0 all-gather.4.cloned.1.call-start
  80.0 0.0 copy-done.6
  80.1 0.1 constant_dynamic-slice_fusion
  80.1 0.0 copy-done.5
  80.2 0.1 copy.42
  80.3 0.1 copy.41
  80.4 23.1 %reduce-scatter.3.cloned.1.call-done = bf16[64,2048]{1,0:T(8,128)(2,1)} async-done(((bf16[256,2048]{1,0:T(8,128)(2,1)}), bf16[64,2048]{1,0:T(8,128)(2,1)}) %reduce-scatter.3.cloned.1.call-update) | async-done | bytes 262160 | tf_op jit(solution)/shard_map/reduce_scatter | solution.py:206
  103.5 0.0 copy-done.1
  103.5 1.1 multiply_reduce_fusion
  104.6 0.0 copy-done.4
  104.6 1.1 multiply_convert_fusion.2
  105.7 0.8 concatenate.11
  106.5 0.0 all-gather.4.cloned.1.call-update
  106.6 0.0 reduce-scatter.5.cloned.1.call-start
  106.6 79.2 %all-gather.4.cloned.1.call-done = bf16[2048,2176]{1,0:T(8,128)(2,1)} async-done(((bf16[64,2176]{1,0:T(8,128)(2,1)}), bf16[2048,2176]{1,0:T(8,128)(2,1)}) %all-gather.4.cloned.1.call-update) | async-done | bytes 8912912 | tf_op jit(solution)/shard_map/all_gather | solution.py:167
  185.9 1.3 select_reduce_fusion
  187.1 10.5 %fusion = f32[2048,512]{1,0:T(8,128)} fusion(bf16[2048,2176]{1,0:T(8,128)(2,1)} %all-gather.4.cloned.1.call-done, bf16[1,2048,512]{2,1,0:T(8,128)(2,1)} %param.23), kind=kOutput, calls=%fused_computation.1 | convolution fusion | flops 4294967296 | bytes 14680064 | tf_op jit(solution)/shard_map/dot_general | solution.py:35
  197.6 0.0 copy-done
  197.6 15.2 %multiply_convert_fusion = bf16[2048,2048]{1,0:T(8,128)(2,1)} fusion(f32[2048]{0:T(1024)S(1)} %select_reduce_fusion, bf16[1,512,2048]{2,1,0:T(8,128)(2,1)S(1)} %copy-done, f32[2048,512]{1,0:T(8,128)} %fusion, bf16[2048,2176]{1,0:T(8,128)(2,1)} %all-gather.4.cloned.1.call-done, bf16[1,2048,512]{2,1,0:T(8,128)(2,1)} %param.24), kind=kOutput, calls=%fused_computation | convolution fusion | flops 8608808960 | bytes 25174016 | tf_op jit(solution)/shard_map/dot_general | solution.py:175
  212.8 0.0 copy-start.2
  212.8 0.0 reduce-scatter.5.cloned.1.call-update
  212.8 149.0 %reduce-scatter.5.cloned.1.call-done = bf16[64,2048]{1,0:T(8,128)(2,1)} async-done(((bf16[2048,2048]{1,0:T(8,128)(2,1)}), bf16[64,2048]{1,0:T(8,128)(2,1)}) %reduce-scatter.5.cloned.1.call-update) | async-done | bytes 262160 | tf_op jit(solution)/shard_map/reduce_scatter | solution.py:176
  361.9 0.0 copy-done.2
  361.9 1.7 add_convert_fusion
  (12 shorter events, 0.1 us)
Async XLA Ops:
  6.5 191.1 %copy-start = (bf16[1,512,2048]{2,1,0:T(8,128)(2,1)S(1)}, bf16[1,512,2048]{2,1,0:T(8,128)(2,1)}, u32[]{:S(2)}) copy-start(bf16[1,512,2048]{2,1,0:T(8,128)(2,1)} %param.25) | copy-start | bytes 6291460
  6.5 62.3 %all-gather.6.cloned.1.call-start = ((), (), s32[]{:S(2)}) async-start(), calls=%async_computation.5 | async-start | bytes 2506752 | tf_op jit(solution)/shard_map/all_gather | solution.py:136
  9.0 2.2 copy-start.3
  15.5 87.9 %reduce-scatter.3.cloned.1.call-start = ((), (), s32[]{:S(2)}) async-start(), calls=%async_computation.2 | async-start | bytes 1310720 | tf_op jit(solution)/shard_map/reduce_scatter | solution.py:206
  70.0 10.0 %copy-start.6 = (s32[256,4]{0,1:T(4,128)S(1)}, s32[256,4]{0,1:T(4,128)}, u32[]{:S(2)}) copy-start(s32[256,4]{0,1:T(4,128)} %param.26) | copy-start | bytes 12292
  70.0 10.1 %copy-start.5 = (f32[64,4]{0,1:T(4,128)S(1)}, f32[64,4]{0,1:T(4,128)}, u32[]{:S(2)}) copy-start(f32[64,4]{0,1:T(4,128)} %param.27) | copy-start | bytes 3076
  70.0 33.5 %copy-start.1 = (bf16[64,2048]{1,0:T(8,128)(2,1)S(1)}, bf16[64,2048]{1,0:T(8,128)(2,1)}, u32[]{:S(2)}) copy-start(bf16[64,2048]{1,0:T(8,128)(2,1)} %param.21) | copy-start | bytes 786436
  70.0 34.6 %copy-start.4 = (f32[2048]{0:T(1024)S(1)}, f32[2048]{0:T(1024)}, u32[]{:S(2)}) copy-start(f32[2048]{0:T(1024)} %param.22) | copy-start | bytes 24580
  80.0 105.9 %all-gather.4.cloned.1.call-start = ((), (), s32[]{:S(2)}) async-start(), calls=%async_computation.3 | async-start | bytes 9191424 | tf_op jit(solution)/shard_map/all_gather | solution.py:167
  106.6 255.3 %reduce-scatter.5.cloned.1.call-start = ((), (), s32[]{:S(2)}) async-start(), calls=%async_computation.4 | async-start | bytes 8650752 | tf_op jit(solution)/shard_map/reduce_scatter | solution.py:176
  212.8 149.0 %copy-start.2 = (bf16[64,2048]{1,0:T(8,128)(2,1)S(1)}, bf16[64,2048]{1,0:T(8,128)(2,1)}, u32[]{:S(2)}) copy-start(bf16[64,2048]{1,0:T(8,128)(2,1)} %reduce-scatter.3.cloned.1.call-done) | copy-start | bytes 786436
Sparse Core Ops, SparseCore 0:
  15.7 53.0 all-gather.5
  80.1 23.3 reduce-scatter.2
  106.7 79.1 all-gather.3
  213.0 148.8 reduce-scatter.4

commit v2 on v1

--- a/solution.py
+++ b/solution.py
@@ -155,6 +155,217 @@
     )(retained, qdec, entering, head_gain[None, :], gate_rows)
 
 
+Z_A, Z_B, X_A2, Y_B2, Y_A3, Y_A4, X_B3, X_B4, C_A, C_B, C_P, Y_A, X_B, X_A, Y_B, RZ_A, RZ_B = range(17)
+
+
+def experts_kernel(
+    planes, x0, x1, upd, wg, wu, wd, out,
+    g0, g1, pm, pc, pr, a0, a1, r10, r11, b0, b1, r20, r21, d0, d1, z0, z1,
+    ssem, rsem, lsem,
+):
+    sp, tp = lax.axis_index("sp"), lax.axis_index("tp")
+    sp_count = 2 * planes
+    z, x = sp // 2, sp % 2
+    y, c = tp // 2, tp % 2
+    half = x1.shape[1]
+    rows = x1.shape[0]
+    f32, bf16 = jnp.float32, jnp.bfloat16
+    to_core = {"sp": sp, "tp": y * 2 + (1 - c)}
+    to_y = {"sp": sp, "tp": (1 - y) * 2 + c}
+    to_x = {"sp": z * 2 + (1 - x), "tp": tp}
+
+    def plane_of(i):
+        return (z + planes - i) % planes
+
+    def to_z(i):
+        return {"sp": plane_of(i) * 2 + x, "tp": tp}
+
+    def from_z(i):
+        return {"sp": ((z + i) % planes) * 2 + x, "tp": tp}
+
+    def move(kind, i, src, dst, device):
+        return pltpu.make_async_remote_copy(
+            src_ref=src, dst_ref=dst, send_sem=ssem.at[kind, i], recv_sem=rsem.at[kind, i],
+            device_id=device, device_id_type=pl.DeviceIdType.MESH,
+        )
+
+    def send(kind, i, src, dst, device):
+        move(kind, i, src, dst, device).start()
+
+    def arrived(kind, i, dst):
+        move(kind, i, dst, dst, to_core).wait_recv()
+
+    def left(kind, i, src):
+        move(kind, i, src, src, to_core).wait_send()
+
+    barrier = pltpu.get_barrier_semaphore()
+    for device in [to_core, to_y, to_x] + [to_z(i) for i in range(1, planes)]:
+        pl.semaphore_signal(barrier, inc=1, device_id=device, device_id_type=pl.DeviceIdType.MESH)
+    pl.semaphore_wait(barrier, 2 + planes)
+
+    here = x * 2 + y
+    other_x = (1 - x) * 2 + y
+    other_y = x * 2 + (1 - y)
+    other_xy = (1 - x) * 2 + (1 - y)
+    own0 = pltpu.make_async_copy(x0, g0.at[c, z, here], lsem.at[0])
+    own1 = pltpu.make_async_copy(x1, g1.at[c, z, here], lsem.at[1])
+    own0.start()
+    own1.start()
+    own0.wait()
+    own1.wait()
+    for i in range(1, planes):
+        send(Z_A, i, g0.at[c, z, here], g0.at[c, z, here], from_z(i))
+        send(Z_B, i, g1.at[c, z, here], g1.at[c, z, here], from_z(i))
+
+    def compute(i, core):
+        p = plane_of(i)
+        left_rows = g0[core, p].reshape(4 * rows, half + 128)
+        right_rows = g1[core, p].reshape(4 * rows, half)
+        tail = left_rows[:, half:].astype(f32)
+        left_rows = left_rows[:, :half]
+        lane = lax.broadcasted_iota(jnp.int32, tail.shape, 1)
+        weight = jnp.sum(
+            jnp.where((lane == sp) | (lane == sp + sp_count), tail, 0.0), axis=1, keepdims=True
+        )
+
+        def product(w):
+            return jnp.dot(left_rows, w[:half, :], preferred_element_type=f32) + jnp.dot(
+                right_rows, w[half:, :], preferred_element_type=f32
+            )
+
+        gate = jnp.minimum(product(wg), clamp_limit)
+        up = jnp.clip(product(wu), -clamp_limit, clamp_limit)
+        act = ((up + 1.0) * (gate / (1.0 + jnp.exp(-swish_alpha * gate)))).astype(bf16)
+        return (jnp.dot(act, wd[...], preferred_element_type=f32) * weight).astype(bf16)
+
+    def step(i, carry):
+        @pl.when((i >= 1) & (i < planes + 1))
+        def _():
+            j = i - 1
+            p = plane_of(j)
+            arrived(Y_A3, j, g0.at[c, p, other_y])
+            arrived(Y_A4, j, g0.at[c, p, other_xy])
+            arrived(X_B3, j, g1.at[c, p, other_x])
+            arrived(X_B4, j, g1.at[c, p, other_xy])
+            send(C_A, j, g0.at[c, p], g0.at[c, p], to_core)
+            send(C_B, j, g1.at[c, p], g1.at[c, p], to_core)
+
+        @pl.when(i < planes)
+        def _():
+            p = plane_of(i)
+
+            @pl.when(i > 0)
+            def _():
+                arrived(Z_A, i, g0.at[c, p, here])
+                arrived(Z_B, i, g1.at[c, p, here])
+
+            send(X_A2, i, g0.at[c, p, here], g0.at[c, p, here], to_x)
+            send(Y_B2, i, g1.at[c, p, here], g1.at[c, p, here], to_y)
+            send(Y_A3, i, g0.at[c, p, here], g0.at[c, p, here], to_y)
+            send(X_B3, i, g1.at[c, p, here], g1.at[c, p, here], to_x)
+            arrived(X_A2, i, g0.at[c, p, other_x])
+            send(Y_A4, i, g0.at[c, p, other_x], g0.at[c, p, other_x], to_y)
+            arrived(Y_B2, i, g1.at[c, p, other_y])
+            send(X_B4, i, g1.at[c, p, other_y], g1.at[c, p, other_y], to_x)
+
+        @pl.when((i >= 2) & (i < planes + 2))
+        def _():
+            j = i - 2
+            arrived(C_P, j, pr.at[j])
+            for q in range(4):
+                part = pl.ds(q * rows, rows)
+                total = (pm[j, part, :].astype(f32) + pr[j, part, :].astype(f32)).astype(bf16)
+                a0[j, q % 2, q // 2] = total[:, :half]
+                a1[j, q // 2, q % 2] = total[:, half:]
+            send(Y_A, j, a0.at[j, 1 - y], r10.at[j], to_y)
+            send(X_B, j, a1.at[j, 1 - x], r11.at[j], to_x)
+
+        @pl.when((i >= 3) & (i < planes + 3))
+        def _():
+            j = i - 3
+            arrived(Y_A, j, r10.at[j])
+            b0[j] = (a0[j, y].astype(f32) + r10[j].astype(f32)).astype(bf16)
+            send(X_A, j, b0.at[j, 1 - x], r20.at[j], to_x)
+            arrived(X_B, j, r11.at[j])
+            b1[j] = (a1[j, x].astype(f32) + r11[j].astype(f32)).astype(bf16)
+            send(Y_B, j, b1.at[j, 1 - y], r21.at[j], to_y)
+
+        @pl.when((i >= 4) & (i < planes + 4))
+        def _():
+            j = i - 4
+            arrived(X_A, j, r20.at[j])
+            d0[j] = (b0[j, x].astype(f32) + r20[j].astype(f32)).astype(bf16)
+            arrived(Y_B, j, r21.at[j])
+            d1[j] = (b1[j, y].astype(f32) + r21[j].astype(f32)).astype(bf16)
+
+            @pl.when(j > 0)
+            def _():
+                send(RZ_A, j, d0.at[j], z0.at[j], to_z(j))
+                send(RZ_B, j, d1.at[j], z1.at[j], to_z(j))
+
+        @pl.when((i >= 1) & (i < planes + 1))
+        def _():
+            j = i - 1
+            p = plane_of(j)
+            arrived(C_A, j, g0.at[1 - c, p])
+            arrived(C_B, j, g1.at[1 - c, p])
+
+            def tile(turn, carry):
+                @pl.when(turn == 0)
+                def _():
+                    pc[j] = compute(j, 1 - c)
+                    send(C_P, j, pc.at[j], pr.at[j], to_core)
+
+                @pl.when(turn == 1)
+                def _():
+                    pm[j] = compute(j, c)
+
+                return carry
+
+            lax.fori_loop(0, 2, tile, 0)
+
+        return carry
+
+    lax.fori_loop(0, planes + 4, step, 0)
+    low, high = upd[:, :half], upd[:, half:]
+    low = low + d0[0].astype(f32)
+    high = high + d1[0].astype(f32)
+    for i in range(1, planes):
+        arrived(RZ_A, i, z0.at[i])
+        low = low + z0[i].astype(f32)
+        arrived(RZ_B, i, z1.at[i])
+        high = high + z1[i].astype(f32)
+    out[:, :half] = low.astype(bf16)
+    out[:, half:] = high.astype(bf16)
+
+    def drain(i, carry):
+        p = plane_of(i)
+
+        @pl.when(i > 0)
+        def _():
+            left(Z_A, i, g0.at[c, z, here])
+            left(Z_B, i, g1.at[c, z, here])
+            left(RZ_A, i, d0.at[i])
+            left(RZ_B, i, d1.at[i])
+
+        left(X_A2, i, g0.at[c, p, here])
+        left(Y_B2, i, g1.at[c, p, here])
+        left(Y_A3, i, g0.at[c, p, here])
+        left(X_B3, i, g1.at[c, p, here])
+        left(Y_A4, i, g0.at[c, p, other_x])
+        left(X_B4, i, g1.at[c, p, other_y])
+        left(C_A, i, g0.at[c, p])
+        left(C_B, i, g1.at[c, p])
+        left(C_P, i, pc.at[i])
+        left(Y_A, i, a0.at[i, 1 - y])
+        left(X_B, i, a1.at[i, 1 - x])
+        left(X_A, i, b0.at[i, 1 - x])
+        left(Y_B, i, b1.at[i, 1 - y])
+        return carry
+
+    lax.fori_loop(0, planes, drain, 0)
+
+
 def dense_experts(updated, ffn_in, own_routes, route_weights, gate_part, up_part, down_part):
     sp_count, mine = lax.axis_size("sp"), lax.axis_index("sp")
     width = ffn_in.shape[1]
@@ -163,20 +374,44 @@
     coarse = shares.astype(jnp.bfloat16)
     fine = (shares - coarse.astype(jnp.float32)).astype(jnp.bfloat16)
     spare = jnp.zeros((ffn_in.shape[0], 128 - 2 * sp_count), jnp.bfloat16)
-    payload = jnp.concatenate([ffn_in, coarse, fine, spare], axis=1)
-    everyone = lax.all_gather(payload, ("sp", "tp"), axis=0, tiled=True)
-    rows = everyone[:, :width]
-    tail = everyone[:, width:].astype(jnp.float32)
-    lane = jnp.arange(128, dtype=jnp.int32)[None, :]
-    weight = jnp.sum(
-        jnp.where((lane == mine) | (lane == mine + sp_count), tail, 0.0), axis=1, keepdims=True
-    )
-    activity = expert_rows(rows, gate_part, up_part)
-    partial_out = jnp.dot(activity, down_part, preferred_element_type=jnp.float32) * weight
-    summed = lax.psum_scatter(
-        partial_out.astype(jnp.bfloat16), ("sp", "tp"), scatter_dimension=0, tiled=True
-    )
-    return (updated + summed.astype(jnp.float32)).astype(jnp.bfloat16)
+    half = width // 2
+    first = jnp.concatenate([ffn_in[:, :half], coarse, fine, spare], axis=1)
+    second = ffn_in[:, half:]
+    rows = ffn_in.shape[0]
+    planes = sp_count // 2
+    bf16 = jnp.bfloat16
+    whole = pl.BlockSpec(memory_space=pltpu.VMEM)
+    return pl.pallas_call(
+        functools.partial(experts_kernel, planes),
+        out_shape=jax.ShapeDtypeStruct((rows, width), bf16),
+        in_specs=[whole] * 6,
+        out_specs=whole,
+        scratch_shapes=[
+            pltpu.VMEM((2, planes, 4, rows, half + 128), bf16),
+            pltpu.VMEM((2, planes, 4, rows, half), bf16),
+            pltpu.VMEM((planes, 4 * rows, width), bf16),
+            pltpu.VMEM((planes, 4 * rows, width), bf16),
+            pltpu.VMEM((planes, 4 * rows, width), bf16),
+            pltpu.VMEM((planes, 2, 2, rows, half), bf16),
+            pltpu.VMEM((planes, 2, 2, rows, half), bf16),
+            pltpu.VMEM((planes, 2, rows, half), bf16),
+            pltpu.VMEM((planes, 2, rows, half), bf16),
+            pltpu.VMEM((planes, 2, rows, half), bf16),
+            pltpu.VMEM((planes, 2, rows, half), bf16),
+            pltpu.VMEM((planes, rows, half), bf16),
+            pltpu.VMEM((planes, rows, half), bf16),
+            pltpu.VMEM((planes, rows, half), bf16),
+            pltpu.VMEM((planes, rows, half), bf16),
+            pltpu.VMEM((planes, rows, half), bf16),
+            pltpu.VMEM((planes, rows, half), bf16),
+            pltpu.SemaphoreType.DMA((17, planes)),
+            pltpu.SemaphoreType.DMA((17, planes)),
+            pltpu.SemaphoreType.DMA((2,)),
+        ],
+        compiler_params=pltpu.CompilerParams(
+            collective_id=0, has_side_effects=True, vmem_limit_bytes=63 * 1024 * 1024
+        ),
+    )(first, second, updated, gate_part, up_part, down_part)
 
 
 def body(
@@ -213,7 +448,7 @@
     ffn_in = square_norm(updated, ffn_gain)
     tp_index = lax.axis_index("tp")
     own_routes = lax.dynamic_slice_in_dim(routes, tp_index * rows_own, rows_own, 0)
-    if rows_own < 2 * capacity and 2 * sp_count <= 128:
+    if rows_own < 2 * capacity and 2 * sp_count <= 128 and sp_count % 2 == 0 and tp_count == 4:
         return dense_experts(
             updated, ffn_in, own_routes, route_weights, gate_weight[0], up_weight[0], down_weight[0]
         )

time: 371 us -> 220 us (0.59)
  waiting for transfers between devices: 305 us -> 76.3 us
  Pallas kernels: 8.27 us -> 112 us
  matrix products: 29.1 us -> 2.73 us
    reduce_scatter x1 -> x0, waiting for transfers between devices: 149 us -> none  [dense_experts(): lax.psum_scatter(partial_out.astype(jnp.bfloat16), ('sp', 'tp'), scatter_...]
    pallas_call x0 -> x1, Pallas kernels: none -> 104 us  [dense_experts(): pl.pallas_call(functools.partial(experts_kernel, planes), out_shape=jax.S...]
    all_gather x1 -> x0, waiting for transfers between devices: 79.2 us -> none  [dense_experts(): everyone = lax.all_gather(payload, ('sp', 'tp'), axis=0, tiled=True)]
    dot_general x2 -> x0, matrix products: 25.7 us -> none  [the longest x1 15.2 us: dense_experts(): jnp.dot(activity, down_part, preferred_element_type=jnp.float32) * weight]
  transfers between devices with their start and end apart: 4 -> 2, of which waited for: 4 -> 2; matrix products, arithmetic and copies ran while one was open for 0% -> 0% of each run, Pallas kernels for 0% -> 0%
where the time goes in v2:
time: 220 us
  Pallas kernels  112 us (51%)
  waiting for transfers between devices  76.3 us (35%)
  between operations  13.5 us (6%)
  other arithmetic  8.39 us (4%)
  local copies, waits for them, and re-layouts  6.37 us (3%)
  matrix products  2.73 us (1%)
    pallas_call x1, Pallas kernels, dense_experts(): pl.pallas_call(functools.partial(experts_kernel, planes), out_shape=jax.S...  104 us
    all_gather x1, waiting for transfers between devices, retention(): pieces = lax.all_gather(state, 'sp')  53.2 us
    reduce_scatter x1, waiting for transfers between devices, body(): lax.psum_scatter(jnp.dot(hidden, out_weight, preferred_element_type=jnp.f...  23.1 us
  transfers between devices with their start and end apart: 2, of which 2 were waited for; matrix products, arithmetic and copies ran while one was open for 0% of the time, Pallas kernels for 0%

profile of v2, /device:TPU:0, one launch (start us, length us, event | category | flops | bytes accessed | tf_op | source)
XLA Modules:
  0.0 219.7 jit_solution(18215648511490937368)
XLA Ops:
  6.5 0.0 copy-start
  6.5 0.0 all-gather.3.cloned.1.call-start
  6.6 0.7 reshape.98
  7.3 1.2 reduce-window.6
  8.5 0.1 slice.24
  8.6 0.1 copy.36
  8.7 0.1 copy.37
  8.8 0.1 broadcast_add_fusion
  8.9 0.0 copy-start.3
  8.9 0.8 copy.38
  9.7 0.5 fusion.1
  10.2 0.8 pad_maximum_fusion
  11.1 0.0 copy-done.3
  11.1 4.3 %shard_map.136 = (f32[256,512]{1,0:T(8,128)}, bf16[256,512]{1,0:T(8,128)(2,1)}, f32[4,136,128]{2,1,0:T(8,128)}) custom-call(bf16[256,512]{1,0:T(8,128)(2,1)} %q_ref.1, bf16[256,512]{1,0:T(8,128)(2,1)} %k_ref.1, bf16[256,512]{1,0:T(8,128)(2,1)} %v_ref.1, f32[256,128]{1,0:T(8,128)} %get-tuple-element.18.cos_ref, f32[256,128]{1,0:T(8,128)} %get-tuple-element.19.sin_ref, ...), custom_call_target="tpu_custom_call" | custom-call | tf_op jit(solution)/shard_map/pallas_call | solution.py:113
  15.4 0.0 copy-start.1
  15.4 0.0 all-gather.3.cloned.1.call-update
  15.4 0.0 reduce-scatter.2.cloned.1.call-start
  15.5 53.2 %all-gather.3.cloned.1.call-done = f32[32,136,128]{2,1,0:T(8,128)} async-done(((f32[4,136,128]{2,1,0:T(8,128)}), f32[32,136,128]{2,1,0:T(8,128)}) %all-gather.3.cloned.1.call-update) | async-done | bytes 2228240 | tf_op jit(solution)/shard_map/all_gather | solution.py:136
  68.7 0.9 slice.25
  69.6 0.1 copy.44
  69.7 0.1 select_reduce_fusion.1
  69.8 0.1 copy.40
  69.9 2.6 %fusion.enter_ref = f32[4,128,128]{2,1,0:T(8,128)} fusion(f32[8,4,136,128]{3,2,1,0:T(8,128)} %bitcast.18, f32[8,4]{1,0:T(8,128)S(1)} %copy.40), kind=kLoop, calls=%fused_computation.2 | loop fusion | flops 983040 | bytes 2359424 | tf_op jit(solution)/shard_map/reduce_sum | solution.py:142
  72.4 4.0 %shard_map.137 = bf16[256,512]{1,0:T(8,128)(2,1)} custom-call(f32[256,512]{1,0:T(8,128)} %get-tuple-element.8.ret_ref, bf16[256,512]{1,0:T(8,128)(2,1)} %get-tuple-element.9.qdec_ref, f32[4,128,128]{2,1,0:T(8,128)} %fusion.enter_ref, f32[1,512]{1,0:T(1,128)} %bitcast.24, bf16[256,512]{1,0:T(8,128)(2,1)} %gate_ref.1), custom_call_target="tpu_custom_call" | custom-call | tf_op jit(solution)/shard_map/pallas_call | solution.py:143
  76.4 0.0 copy-done.1
  76.4 0.0 copy-start.5
  76.4 0.0 copy-start.2
  76.4 0.0 copy-start.4
  76.4 2.7 %convolution_convert_fusion = bf16[256,2048]{1,0:T(8,128)(2,1)} fusion(bf16[256,512]{1,0:T(8,128)(2,1)} %shard_map.137, bf16[512,2048]{1,0:T(8,128)(2,1)S(1)} %copy-done.1), kind=kOutput, calls=%fused_computation | convolution fusion | flops 537395200 | bytes 3407872 | tf_op jit(solution)/shard_map/dot_general | solution.py:442
  79.2 0.0 reduce-scatter.2.cloned.1.call-update
  79.2 0.0 copy-done
  79.2 0.1 constant_dynamic-slice_fusion
  79.3 0.0 copy-done.5
  79.3 0.1 copy.41
  79.4 0.1 copy.43
  79.5 0.1 copy.42
  79.6 23.1 %reduce-scatter.2.cloned.1.call-done = bf16[64,2048]{1,0:T(8,128)(2,1)} async-done(((bf16[256,2048]{1,0:T(8,128)(2,1)}), bf16[64,2048]{1,0:T(8,128)(2,1)}) %reduce-scatter.2.cloned.1.call-update) | async-done | bytes 262160 | tf_op jit(solution)/shard_map/reduce_scatter | solution.py:441
  102.7 0.0 copy-done.2
  102.7 1.9 convert_add_fusion
  104.6 0.0 copy-done.4
  104.6 1.1 multiply_convert_fusion
  105.7 0.7 fusion.3
  106.4 0.8 concatenate.11.x0
  107.1 104.0 %shard_map.138 = bf16[64,2048]{1,0:T(8,128)(2,1)} custom-call(bf16[64,1152]{1,0:T(8,128)(2,1)} %concatenate.11.x0, bf16[64,1024]{1,0:T(8,128)(2,1)} %get-tuple-element.13.x1, f32[64,2048]{1,0:T(8,128)} %get-tuple-element.11.upd, bf16[2048,512]{1,0:T(8,128)(2,1)} %bitcast.14, bf16[2048,512]{1,0:T(8,128)(2,1)} %bitcast.15, bf16[512,2048]{1,0:T(8,128)(2,1)} %bitcast.16), custom_call_target="tpu_custom_call" | custom-call | tf_op jit(solution)/shard_map/pallas_call | solution.py:384
  211.1 1.7 copy.46
  (12 shorter events, 0.1 us)
Async XLA Ops:
  6.5 72.6 %copy-start = (s32[256,4]{0,1:T(4,128)S(1)}, s32[256,4]{0,1:T(4,128)}, u32[]{:S(2)}) copy-start(s32[256,4]{0,1:T(4,128)} %param.26) | copy-start | bytes 12292
  6.5 62.1 %all-gather.3.cloned.1.call-start = ((), (), s32[]{:S(2)}) async-start(), calls=%async_computation.2 | async-start | bytes 2506752 | tf_op jit(solution)/shard_map/all_gather | solution.py:136
  8.9 2.2 copy-start.3
  15.4 61.0 %copy-start.1 = (bf16[512,2048]{1,0:T(8,128)(2,1)S(1)}, bf16[512,2048]{1,0:T(8,128)(2,1)}, u32[]{:S(2)}) copy-start(bf16[512,2048]{1,0:T(8,128)(2,1)} %param.20) | copy-start | bytes 6291460
  15.4 87.3 %reduce-scatter.2.cloned.1.call-start = ((), (), s32[]{:S(2)}) async-start(), calls=%async_computation.1 | async-start | bytes 1310720 | tf_op jit(solution)/shard_map/reduce_scatter | solution.py:441
  76.4 2.9 %copy-start.5 = (f32[64,4]{0,1:T(4,128)S(1)}, f32[64,4]{0,1:T(4,128)}, u32[]{:S(2)}) copy-start(f32[64,4]{0,1:T(4,128)} %param.27) | copy-start | bytes 3076
  76.4 26.3 %copy-start.2 = (bf16[64,2048]{1,0:T(8,128)(2,1)S(1)}, bf16[64,2048]{1,0:T(8,128)(2,1)}, u32[]{:S(2)}) copy-start(bf16[64,2048]{1,0:T(8,128)(2,1)} %param.21) | copy-start | bytes 786436
  76.4 28.2 %copy-start.4 = (f32[2048]{0:T(1024)S(1)}, f32[2048]{0:T(1024)}, u32[]{:S(2)}) copy-start(f32[2048]{0:T(1024)} %param.22) | copy-start | bytes 24580
Sparse Core Ops, SparseCore 0:
  15.5 53.0 all-gather.2
  79.3 23.3 reduce-scatter.1

commit v3 on v2

--- a/solution.py
+++ b/solution.py
@@ -96,6 +96,105 @@
     gate = gate_ref[...].astype(jnp.float32)
     scaled = centred * lax.rsqrt(variance + group_eps) * gain_ref[...]
     hidden_ref[...] = (scaled * (gate / (1.0 + jnp.exp(-gate)))).astype(jnp.bfloat16)
+
+
+def greet(devices):
+    barrier = pltpu.get_barrier_semaphore()
+    for device in devices:
+        pl.semaphore_signal(barrier, inc=1, device_id=device, device_id_type=pl.DeviceIdType.MESH)
+    pl.semaphore_wait(barrier, len(devices))
+
+
+def state_kernel(planes, state, totals, entering, gs, gt, ssem, rsem, lsem):
+    sp, tp = lax.axis_index("sp"), lax.axis_index("tp")
+    z, x = sp // 2, sp % 2
+    heads = state.shape[0]
+    to_x = {"sp": z * 2 + (1 - x), "tp": tp}
+
+    def later(i):
+        return {"sp": ((z + i) % planes) * 2 + x, "tp": tp}
+
+    def plane_of(i):
+        return (z + planes - i) % planes
+
+    def move(kind, i, ref, device):
+        return pltpu.make_async_remote_copy(
+            src_ref=ref, dst_ref=ref, send_sem=ssem.at[kind, i], recv_sem=rsem.at[kind, i],
+            device_id=device, device_id_type=pl.DeviceIdType.MESH,
+        )
+
+    own = [
+        pltpu.make_async_copy(state, gs.at[z, x], lsem.at[0]),
+        pltpu.make_async_copy(totals, gt.at[z, x], lsem.at[1]),
+    ]
+    for copy in own:
+        copy.start()
+    greet([to_x] + [later(i) for i in range(1, planes)])
+    for copy in own:
+        copy.wait()
+    for i in range(1, planes):
+        move(0, i, gs.at[z, x], later(i)).start()
+        move(1, i, gt.at[z, x], later(i)).start()
+    for i in range(planes):
+        p = plane_of(i)
+        if i > 0:
+            move(0, i, gs.at[p, x], to_x).wait_recv()
+            move(1, i, gt.at[p, x], to_x).wait_recv()
+        move(2, i, gs.at[p, x], to_x).start()
+        move(3, i, gt.at[p, x], to_x).start()
+    for i in range(planes):
+        p = plane_of(i)
+        move(2, i, gs.at[p, 1 - x], to_x).wait_recv()
+        move(3, i, gt.at[p, 1 - x], to_x).wait_recv()
+    running = jnp.zeros((8, HEAD_DIM), jnp.float32)
+    sums = [jnp.zeros((HEAD_DIM, HEAD_DIM), jnp.float32) for _ in range(heads)]
+    for s in reversed(range(2 * planes)):
+        earlier = s < sp
+        factor = jnp.where(earlier, jnp.exp(running), 0.0)
+        running = running + jnp.where(earlier, gt[s // 2, s % 2], 0.0)
+        for h in range(heads):
+            sums[h] = sums[h] + factor[h : h + 1, :] * gs[s // 2, s % 2, h].astype(jnp.float32)
+    for h in range(heads):
+        entering[h] = sums[h].astype(jnp.bfloat16)
+    for i in range(planes):
+        p = plane_of(i)
+        if i > 0:
+            move(0, i, gs.at[z, x], to_x).wait_send()
+            move(1, i, gt.at[z, x], to_x).wait_send()
+        move(2, i, gs.at[p, x], to_x).wait_send()
+        move(3, i, gt.at[p, x], to_x).wait_send()
+
+
+def mix_kernel(part, out, from_core, held, from_y, ssem, rsem):
+    sp, tp = lax.axis_index("sp"), lax.axis_index("tp")
+    y, c = tp // 2, tp % 2
+    to_core = {"sp": sp, "tp": y * 2 + (1 - c)}
+    to_y = {"sp": sp, "tp": (1 - y) * 2 + c}
+
+    def move(i, src, dst, device):
+        return pltpu.make_async_remote_copy(
+            src_ref=src, dst_ref=dst, send_sem=ssem.at[i], recv_sem=rsem.at[i],
+            device_id=device, device_id_type=pl.DeviceIdType.MESH,
+        )
+
+    greet([to_core, to_y])
+    far = move(0, part.at[1 - y, 1 - c], from_core.at[0], to_core)
+    near = move(1, part.at[y, 1 - c], from_core.at[1], to_core)
+    far.start()
+    near.start()
+    far.wait_recv()
+    held[0] = (
+        part[1 - y, c].astype(jnp.float32) + from_core[0].astype(jnp.float32)
+    ).astype(jnp.bfloat16)
+    across = move(2, held.at[0], from_y, to_y)
+    across.start()
+    near.wait_recv()
+    mine = part[y, c].astype(jnp.float32) + from_core[1].astype(jnp.float32)
+    across.wait_recv()
+    out[...] = mine + from_y[...].astype(jnp.float32)
+    far.wait_send()
+    near.wait_send()
+    across.wait_send()
 
 
 def retention(query_rows, key_rows, value_rows, gate_rows, log_decay, head_gain):
@@ -133,13 +232,33 @@
             pl.BlockSpec((1, HEAD_DIM + 8, HEAD_DIM), lambda h: (h, 0, 0)),
         ),
     )(query_rows, key_rows, value_rows, cosine, sine, cumulative, cumulative.T[:, None, :])
-    pieces = lax.all_gather(state, "sp")
-    totals = pieces[:, :, HEAD_DIM, 0]
-    index = jnp.arange(sp_count, dtype=jnp.int32)
-    between = (index[None, :] > index[:, None]) & (index[None, :] < mine)
-    gap = jnp.sum(jnp.where(between[:, :, None], totals[None], 0.0), axis=1)
-    factor = jnp.where((index < mine)[:, None], jnp.exp(gap), 0.0)
-    entering = jnp.sum(factor[:, :, None, None] * pieces[:, :, :HEAD_DIM, :], axis=0)
+    if sp_count % 2 == 0 and local_heads <= 8 and sp_count <= 16:
+        totals = jnp.broadcast_to(state[:, HEAD_DIM, :1], (local_heads, HEAD_DIM))
+        totals = jnp.pad(totals, ((0, 8 - local_heads), (0, 0)))
+        planes = sp_count // 2
+        block = (local_heads, HEAD_DIM, HEAD_DIM)
+        entering = pl.pallas_call(
+            functools.partial(state_kernel, planes),
+            out_shape=jax.ShapeDtypeStruct(block, jnp.bfloat16),
+            in_specs=[pl.BlockSpec(memory_space=pltpu.VMEM)] * 2,
+            out_specs=pl.BlockSpec(memory_space=pltpu.VMEM),
+            scratch_shapes=[
+                pltpu.VMEM((planes, 2) + block, jnp.bfloat16),
+                pltpu.VMEM((planes, 2, 8, HEAD_DIM), jnp.float32),
+                pltpu.SemaphoreType.DMA((4, planes)),
+                pltpu.SemaphoreType.DMA((4, planes)),
+                pltpu.SemaphoreType.DMA((2,)),
+            ],
+            compiler_params=pltpu.CompilerParams(collective_id=1, has_side_effects=True),
+        )(state[:, :HEAD_DIM, :].astype(jnp.bfloat16), totals)
+    else:
+        pieces = lax.all_gather(state, "sp")
+        totals = pieces[:, :, HEAD_DIM, 0]
+        index = jnp.arange(sp_count, dtype=jnp.int32)
+        between = (index[None, :] > index[:, None]) & (index[None, :] < mine)
+        gap = jnp.sum(jnp.where(between[:, :, None], totals[None], 0.0), axis=1)
+        factor = jnp.where((index < mine)[:, None], jnp.exp(gap), 0.0)
+        entering = jnp.sum(factor[:, :, None, None] * pieces[:, :, :HEAD_DIM, :], axis=0)
     return pl.pallas_call(
         norm_kernel,
         grid=(local_heads,),
@@ -438,12 +557,26 @@
     rows_own = tok_count // tp_count
     capacity = max(2, 3 * rows_own * TOPK // (2 * sp_count))
     hidden = retention(query_rows, key_rows, value_rows, gate_rows, log_decay, head_gain)
-    mixed_sum = lax.psum_scatter(
-        jnp.dot(hidden, out_weight, preferred_element_type=jnp.float32).astype(jnp.bfloat16),
-        "tp",
-        scatter_dimension=0,
-        tiled=True,
-    ).astype(jnp.float32)
+    mixed = jnp.dot(hidden, out_weight, preferred_element_type=jnp.float32).astype(jnp.bfloat16)
+    if tp_count == 4 and sp_count <= 16:
+        mixed_sum = pl.pallas_call(
+            mix_kernel,
+            out_shape=jax.ShapeDtypeStruct((rows_own, model_width), jnp.float32),
+            in_specs=[pl.BlockSpec(memory_space=pltpu.VMEM)],
+            out_specs=pl.BlockSpec(memory_space=pltpu.VMEM),
+            scratch_shapes=[
+                pltpu.VMEM((2, rows_own, model_width), jnp.bfloat16),
+                pltpu.VMEM((2, rows_own, model_width), jnp.bfloat16),
+                pltpu.VMEM((rows_own, model_width), jnp.bfloat16),
+                pltpu.SemaphoreType.DMA((3,)),
+                pltpu.SemaphoreType.DMA((3,)),
+            ],
+            compiler_params=pltpu.CompilerParams(collective_id=2, has_side_effects=True),
+        )(mixed.reshape(2, 2, rows_own, model_width))
+    else:
+        mixed_sum = lax.psum_scatter(mixed, "tp", scatter_dimension=0, tiled=True).astype(
+            jnp.float32
+        )
     updated = residual.astype(jnp.float32) + mixed_sum
     ffn_in = square_norm(updated, ffn_gain)
     tp_index = lax.axis_index("tp")

time: 220 us -> 166 us (0.75)
  waiting for transfers between devices: 76.3 us -> 0 us
  Pallas kernels: 112 us -> 151 us
  between operations: 13.5 us -> 0.11 us
  other arithmetic: 8.39 us -> 4.08 us
    all_gather x1 -> x0, waiting for transfers between devices: 53.2 us -> none  [retention(): pieces = lax.all_gather(state, 'sp')]
    pallas_call x0 -> x2, Pallas kernels: none -> 37.4 us  [the longest x1 25.1 us: retention(): pl.pallas_call(functools.partial(state_kernel, planes), out_shape=jax.Sha...]
    reduce_scatter x1 -> x0, waiting for transfers between devices: 23.1 us -> none  [body(): lax.psum_scatter(jnp.dot(hidden, out_weight, preferred_element_type=jnp.f...]
  transfers between devices with their start and end apart: 2 -> 0, of which waited for: 2 -> 0; matrix products, arithmetic and copies ran while one was open for 0% -> 0% of each run, Pallas kernels for 0% -> 0%
where the time goes in v3:
time: 166 us
  Pallas kernels  151 us (91%)
  local copies, waits for them, and re-layouts  8.38 us (5%)
  other arithmetic  4.08 us (2%)
  matrix products  2.73 us (2%)
    pallas_call x1, Pallas kernels, dense_experts(): pl.pallas_call(functools.partial(experts_kernel, planes), out_shape=jax.S...  105 us
    pallas_call x1, Pallas kernels, retention(): pl.pallas_call(functools.partial(state_kernel, planes), out_shape=jax.Sha...  25.1 us
    pallas_call x1, Pallas kernels, body(): pl.pallas_call(mix_kernel, out_shape=jax.ShapeDtypeStruct((rows_own, mode...  12.3 us
    pallas_call x1, Pallas kernels, retention(): pl.pallas_call(retention_kernel, grid=(local_heads,), out_shape=(jax.Shap...  4.35 us
    pallas_call x1, Pallas kernels, retention(): pl.pallas_call(norm_kernel, grid=(local_heads,), out_shape=jax.ShapeDtype...  3.95 us

profile of v3, /device:TPU:0, one launch (start us, length us, event | category | flops | bytes accessed | tf_op | source)
XLA Modules:
  0.0 166.0 jit_solution(16813410180597801080)
XLA Ops:
  0.0 0.0 copy-start
  0.0 0.5 fusion
  0.6 0.0 copy-start.2
  0.6 0.8 pad_maximum_fusion
  1.4 0.7 reshape.49
  2.1 1.2 reduce-window.6
  3.3 0.1 slice.25
  3.4 0.1 copy.30
  3.6 0.1 copy.31
  3.7 0.1 broadcast_add_fusion
  3.7 0.0 copy-start.4
  3.7 0.8 copy.32
  4.5 0.0 copy-done.4
  4.5 4.3 %shard_map.136 = (f32[256,512]{1,0:T(8,128)}, bf16[256,512]{1,0:T(8,128)(2,1)}, f32[4,136,128]{2,1,0:T(8,128)}) custom-call(bf16[256,512]{1,0:T(8,128)(2,1)} %q_ref.1, bf16[256,512]{1,0:T(8,128)(2,1)} %k_ref.1, bf16[256,512]{1,0:T(8,128)(2,1)} %v_ref.1, f32[256,128]{1,0:T(8,128)} %get-tuple-element.18.cos_ref, f32[256,128]{1,0:T(8,128)} %get-tuple-element.19.sin_ref, ...), custom_call_target="tpu_custom_call" | custom-call | tf_op jit(solution)/shard_map/pallas_call | solution.py:212
  8.9 1.6 slice.31.state
  10.5 0.8 slice_reduce_fusion
  11.3 0.6 pad.7.totals
  12.0 25.1 %shard_map.137.enter_ref = bf16[4,128,128]{2,1,0:T(8,128)(2,1)} custom-call(bf16[4,128,128]{2,1,0:T(8,128)(2,1)} %slice.31.state, f32[8,128]{1,0:T(8,128)} %pad.7.totals), custom_call_target="tpu_custom_call" | custom-call | tf_op jit(solution)/shard_map/pallas_call | solution.py:240
  37.1 3.9 %shard_map.138 = bf16[256,512]{1,0:T(8,128)(2,1)} custom-call(f32[256,512]{1,0:T(8,128)} %get-tuple-element.8.ret_ref, bf16[256,512]{1,0:T(8,128)(2,1)} %get-tuple-element.9.qdec_ref, bf16[4,128,128]{2,1,0:T(8,128)(2,1)} %shard_map.137.enter_ref, f32[1,512]{1,0:T(1,128)} %bitcast.21, bf16[256,512]{1,0:T(8,128)(2,1)} %gate_ref.1), custom_call_target="tpu_custom_call" | custom-call | tf_op jit(solution)/shard_map/pallas_call | solution.py:262
  41.1 0.0 copy-done.2
  41.1 0.0 copy-start.3
  41.1 2.7 %convolution_convert_fusion = bf16[256,2048]{1,0:T(8,128)(2,1)} fusion(bf16[256,512]{1,0:T(8,128)(2,1)} %shard_map.138, bf16[512,2048]{1,0:T(8,128)(2,1)S(1)} %copy-done.2), kind=kOutput, calls=%fused_computation | convolution fusion | flops 537395200 | bytes 3407872 | tf_op jit(solution)/shard_map/dot_general | solution.py:560
  43.8 0.0 copy-start.5
  43.8 0.0 copy-start.6
  43.8 12.3 %shard_map.139 = f32[64,2048]{1,0:T(8,128)} custom-call(bf16[2,2,64,2048]{3,2,1,0:T(8,128)(2,1)} %bitcast.13), custom_call_target="tpu_custom_call" | custom-call | tf_op jit(solution)/shard_map/pallas_call | solution.py:562
  56.1 0.0 copy-done.3
  56.1 1.2 multiply_reduce_fusion
  57.3 0.0 copy-start.1
  57.4 0.0 copy-done.5
  57.4 0.1 multiply_convert_fusion
  57.5 0.7 fusion.1
  58.2 0.0 copy-done
  58.2 0.1 constant_dynamic-slice_fusion
  58.2 0.0 copy-done.6
  58.3 0.1 copy.34
  58.4 0.1 copy.33
  58.4 0.1 copy.35
  58.6 0.8 concatenate.11.x0
  59.3 0.0 copy-done.1
  59.3 105.0 %shard_map.140 = bf16[64,2048]{1,0:T(8,128)(2,1)} custom-call(bf16[64,1152]{1,0:T(8,128)(2,1)} %concatenate.11.x0, bf16[64,1024]{1,0:T(8,128)(2,1)} %get-tuple-element.13.x1, f32[64,2048]{1,0:T(8,128)} %copy-done.1, bf16[2048,512]{1,0:T(8,128)(2,1)} %bitcast.14, bf16[2048,512]{1,0:T(8,128)(2,1)} %bitcast.15, bf16[512,2048]{1,0:T(8,128)(2,1)} %bitcast.16), custom_call_target="tpu_custom_call" | custom-call | tf_op jit(solution)/shard_map/pallas_call | solution.py:503
  164.3 1.7 %copy.37 = bf16[64,2048]{1,0:T(8,128)(2,1)} copy(bf16[64,2048]{1,0:T(8,128)(2,1)} %shard_map.140) | data formatting | bytes 524288
  (10 shorter events, 0.1 us)
Async XLA Ops:
  0.0 58.2 %copy-start = (s32[256,4]{0,1:T(4,128)S(1)}, s32[256,4]{0,1:T(4,128)}, u32[]{:S(2)}) copy-start(s32[256,4]{0,1:T(4,128)} %param.26) | copy-start | bytes 12292
  0.6 40.5 %copy-start.2 = (bf16[512,2048]{1,0:T(8,128)(2,1)S(1)}, bf16[512,2048]{1,0:T(8,128)(2,1)}, u32[]{:S(2)}) copy-start(bf16[512,2048]{1,0:T(8,128)(2,1)} %param.20) | copy-start | bytes 6291460
  3.7 0.8 copy-start.4
  41.1 15.0 %copy-start.3 = (bf16[64,2048]{1,0:T(8,128)(2,1)S(1)}, bf16[64,2048]{1,0:T(8,128)(2,1)}, u32[]{:S(2)}) copy-start(bf16[64,2048]{1,0:T(8,128)(2,1)} %param.21) | copy-start | bytes 786436
  43.8 13.5 %copy-start.5 = (f32[2048]{0:T(1024)S(1)}, f32[2048]{0:T(1024)}, u32[]{:S(2)}) copy-start(f32[2048]{0:T(1024)} %param.22) | copy-start | bytes 24580
  43.8 14.4 %copy-start.6 = (f32[64,4]{0,1:T(4,128)S(1)}, f32[64,4]{0,1:T(4,128)}, u32[]{:S(2)}) copy-start(f32[64,4]{0,1:T(4,128)} %param.27) | copy-start | bytes 3076
  57.3 2.0 %copy-start.1 = (f32[64,2048]{1,0:T(8,128)}, f32[64,2048]{1,0:T(8,128)S(1)}, u32[]{:S(2)}) copy-start(f32[64,2048]{1,0:T(8,128)S(1)} %get-tuple-element.12.upd) | copy-start | bytes 1572868
